TPU v7x, 256 devices: a whole 4x4x8 slice. The times are simulated.
256 devices in a mesh: sp: 64 (over z, y, core), tp: 4 (over x).
Axes of the slice: x: 4, y: 4, z: 8, core: 2. Of those that a mesh axis runs over, the one named last changes fastest.
Arguments:
- stream: bfloat16 [8192, 2048], P('sp', 'tp'), may hold values from -40 to 40
- queries: bfloat16 [8192, 1024], P('sp', 'tp'), may hold values from -6 to 6
- keys: bfloat16 [8192, 1024], P('sp', 'tp'), may hold values from -6 to 6
- values: bfloat16 [8192, 2048], P('sp', 'tp'), may hold values from -25 to 25
- out_gate: bfloat16 [8192, 2048], P('sp', 'tp'), may hold values from -8 to 8
- input_gate: float32 [8192, 8], P('sp', 'tp'), may hold values from -9 to 350
- forget_gate: float32 [8192, 8], P('sp', 'tp'), may hold values from -4 to 20
- head_gain: float32 [2048], P('tp'), may hold values from 0.1 to 1.9
- w_out: bfloat16 [2048, 2048], P('tp'), may hold values from -0.125 to 0.125
- ffn_gain: float32 [2048], replicated, may hold values from 0.1 to 1.9
- w_gate: bfloat16 [2048, 5632], P('sp', 'tp'), may hold values from -0.125 to 0.125
- w_up: bfloat16 [2048, 5632], P('sp', 'tp'), may hold values from -0.125 to 0.125
- w_down: bfloat16 [5632, 2048], P('tp', 'sp'), may hold values from -0.078125 to 0.078125
Outputs:
- mixed: bfloat16 [8192, 2048], P('sp', 'tp')
All inputs are finite; a program needn't handle non-finite values.
Results may differ from a plain program's by a relative error of at most 0.0095.
Values may be sent and summed in bfloat16 or wider, within the bound.
A program may use at most 128 MiB of HBM per device.

v0:
```python
import jax
import jax.numpy as jnp
from jax import lax
from jax.sharding import Mesh
from jax.sharding import PartitionSpec as P

D = 2048
DQK = 128
DV = 256
BLOCK = 64
VALS = 2048
SP = ("sp_0", "sp_1", "sp_2")
precise = lax.Precision.HIGHEST
norm_eps = 1e-06
very_low = -1e30


def gather_turned(arrays, axis, dims):
    turned = [jnp.moveaxis(a, dim, 0) for a, dim in zip(arrays, dims)]
    both = jnp.concatenate([t.reshape(len(t), -1) for t in turned], axis=1)
    result, at, gathered = (lax.all_gather(both, axis, axis=0, tiled=True), 0, [])
    for t, dim in zip(turned, dims):
        slab = result[:, at : at + t[0].size].reshape(-1, *t.shape[1:])
        gathered.append(jnp.moveaxis(slab, 0, dim))
        at += t[0].size
    return tuple(gathered)


def nothing_yet(x, identity):
    return jax.tree.map(
        lambda a, e: jnp.broadcast_to(jnp.asarray(e, a.dtype), a.shape), x, identity
    )


def all_in_one(x, axis):
    leaves = jax.tree.leaves(x)
    order = sorted(range(len(leaves)), key=lambda k: -leaves[k].size)
    width = (1, *leaves[order[0]].shape)[-1]
    lines = [
        jnp.pad(leaves[k].reshape(-1), (0, -leaves[k].size % width)).reshape(-1, width)
        for k in order
    ]
    both, at, found = (lax.all_gather(jnp.concatenate(lines), axis), 0, {})
    for k, line in zip(order, lines):
        slab = both[:, at : at + len(line)].reshape(len(both), -1)
        found[k] = slab[:, : leaves[k].size].reshape(-1, *leaves[k].shape)
        at += len(line)
    numbers = iter(range(len(leaves)))
    return jax.tree.map(lambda _: found[next(numbers)], x)


def entering(x, axes, combine, identity):
    before = start = nothing_yet(x, identity)
    subtotal = x
    for axis in reversed(axes):
        peers, mine = (lax.axis_size(axis), lax.axis_index(axis))
        pieces = all_in_one(subtotal, axis)
        inside, subtotal = (start, start)
        for k in range(peers):
            passed = k < mine
            subtotal = combine(subtotal, jax.tree.map(lambda part: part[k], pieces))
            inside = jax.tree.map(lambda new, old: jnp.where(passed, new, old), subtotal, inside)
        before = combine(inside, before)
    return before


def copy_for_each(x, axis):
    peers = lax.axis_size(axis)
    return lax.all_to_all(jnp.broadcast_to(x[None], (peers, *x.shape)), axis, 0, 0, tiled=True)


def over_copies(x, axis):
    everything = copy_for_each(x, axis)
    return jnp.sum(everything, axis=0)


def cut_along(x, dim, peers):
    shape = x.shape
    parts = x.reshape(*shape[:dim], peers, shape[dim] // peers, *shape[dim + 1 :])
    return jnp.moveaxis(parts, dim, 0)


def summed_on_arrival(x, axis, dim):
    parts = cut_along(x, dim, lax.axis_size(axis))
    arrived = lax.all_to_all(parts, axis, split_axis=0, concat_axis=0, tiled=True)
    return arrived.astype(jnp.float32).sum(axis=0)


def in_order(parts, dim):
    shape = list(parts.shape[1:])
    shape[dim] *= parts.shape[0]
    return jnp.moveaxis(parts, 0, dim).reshape(shape)


def gathered_copies(x, axis, dim):
    parts = copy_for_each(x, axis)
    return in_order(parts, dim)


def block_summary(key_blk, value_blk, input_blk, decay_sum):
    decay_total = decay_sum[..., -1]
    log_weight = decay_total[..., None] - decay_sum + input_blk
    weight_peak = jnp.max(log_weight, axis=-1)
    weights = jnp.exp(log_weight - weight_peak[..., None])
    state_mat = jnp.einsum(
        "...ld,...le->...de", weights[..., None] * key_blk, value_blk, precision=precise
    )
    state_vec = jnp.einsum("...l,...ld->...d", weights, key_blk, precision=precise)
    return (state_mat, state_vec, weight_peak, decay_total)


def combine(earlier, later):
    ceiling = jnp.maximum(later[3] + earlier[2], later[2])
    former = jnp.exp(later[3] + earlier[2] - ceiling)
    latter = jnp.exp(later[2] - ceiling)
    return (
        former[..., None, None] * earlier[0] + latter[..., None, None] * later[0],
        former[..., None] * earlier[1] + latter[..., None] * later[1],
        ceiling,
        earlier[3] + later[3],
    )


def block_output(
    query_blk, key_blk, value_blk, input_blk, decay_sum, state_mat, state_vec, state_peak
):
    block_len = query_blk.shape[-2]
    causal = jnp.tril(jnp.ones((block_len, block_len), jnp.bool_))
    log_pair = jnp.where(
        causal,
        decay_sum[..., :, None] - decay_sum[..., None, :] + input_blk[..., None, :],
        -jnp.inf,
    )
    log_carry = decay_sum + state_peak[..., None]
    row_peak = jnp.maximum(log_carry, jnp.max(log_pair, axis=-1))
    scores = jnp.einsum("...ld,...sd->...ls", query_blk, key_blk, precision=precise) * jnp.exp(
        log_pair - row_peak[..., None]
    )
    carried = jnp.exp(log_carry - row_peak)
    numer = jnp.einsum("...ls,...se->...le", scores, value_blk, precision=precise) + carried[
        ..., None
    ] * jnp.einsum("...ld,...de->...le", query_blk, state_mat, precision=precise)
    normer = jnp.sum(scores, axis=-1) + carried * jnp.einsum(
        "...ld,...d->...l", query_blk, state_vec, precision=precise
    )
    denom = jnp.maximum(jnp.abs(normer), jnp.exp(-row_peak))
    return numer / denom[..., None]


def local(
    stream,
    queries,
    keys,
    values,
    out_gate,
    input_gate,
    forget_gate,
    head_gain,
    w_out,
    ffn_gain,
    w_gate,
    w_up,
    w_down,
):
    gate_full, up_full, down_full = gather_turned((w_gate, w_up, w_down), SP, (0, 0, 1))
    count_of_rows = stream.shape[0]
    head_count = input_gate.shape[1]
    blocks = count_of_rows // BLOCK

    def to_blocks(array, col_width):
        return (
            array.astype(jnp.float32)
            .reshape(blocks, BLOCK, head_count, col_width)
            .transpose(2, 0, 1, 3)
        )

    query_blk = to_blocks(queries, DQK) * DQK ** (-0.5)
    key_blk = to_blocks(keys, DQK)
    value_blk = to_blocks(values, DV)
    input_blk = input_gate.reshape(blocks, BLOCK, head_count).transpose(2, 0, 1)
    decay_sum = jnp.cumsum(
        jax.nn.log_sigmoid(forget_gate).reshape(blocks, BLOCK, head_count).transpose(2, 0, 1),
        axis=-1,
    )
    summary = block_summary(key_blk, value_blk, input_blk, decay_sum)
    identity = (
        jnp.zeros((head_count, DQK, DV), jnp.float32),
        jnp.zeros((head_count, DQK), jnp.float32),
        jnp.full((head_count,), very_low, jnp.float32),
        jnp.zeros((head_count,), jnp.float32),
    )

    def advance(carry, piece):
        return (combine(carry, piece), carry)

    local_total, prefix = lax.scan(
        advance, identity, jax.tree.map(lambda array: jnp.moveaxis(array, 1, 0), summary)
    )
    carry_in = entering(local_total, SP, combine, identity)
    start = combine(
        jax.tree.map(lambda array: array[:, None], carry_in),
        jax.tree.map(lambda array: jnp.moveaxis(array, 0, 1), prefix),
    )
    mixed_heads = block_output(
        query_blk, key_blk, value_blk, input_blk, decay_sum, start[0], start[1], start[2]
    )
    head_rows = mixed_heads.transpose(1, 2, 0, 3).reshape(count_of_rows, head_count, DV)
    local_sq = jnp.sum(head_rows * head_rows, axis=(1, 2))
    total_sq = over_copies(local_sq, "tp")
    row_scale = lax.rsqrt(total_sq / VALS + norm_eps)
    gated = (
        head_rows
        * row_scale[:, None, None]
        * head_gain.reshape(head_count, DV)
        * jax.nn.sigmoid(out_gate.astype(jnp.float32).reshape(count_of_rows, head_count, DV))
    )
    heads_out = gated.reshape(count_of_rows, head_count * DV).astype(jnp.bfloat16)
    partial_value = jnp.dot(heads_out, w_out, preferred_element_type=jnp.float32)
    col_width = stream.shape[1]
    col_start = lax.axis_index("tp") * col_width
    mixer_own = summed_on_arrival(partial_value.astype(jnp.bfloat16), "tp", 1)
    resid_own = (stream.astype(jnp.float32) + mixer_own).astype(jnp.bfloat16)
    resid_f = resid_own.astype(jnp.float32)
    square_total = over_copies(jnp.sum(resid_f * resid_f, axis=-1), "tp")
    gain_own = lax.dynamic_slice_in_dim(ffn_gain, col_start, col_width)
    normed_own = (resid_f * lax.rsqrt(square_total / D + norm_eps)[:, None] * gain_own).astype(
        jnp.bfloat16
    )
    normed = gathered_copies(normed_own, "tp", 1)
    gate_act = jnp.dot(normed, gate_full, preferred_element_type=jnp.float32)
    up_act = jnp.dot(normed, up_full, preferred_element_type=jnp.float32)
    hidden = (jax.nn.silu(gate_act) * up_act).astype(jnp.bfloat16)
    term = jnp.dot(hidden, down_full, preferred_element_type=jnp.float32)
    down_own = summed_on_arrival(term.astype(jnp.bfloat16), "tp", 1)
    return (resid_own.astype(jnp.float32) + down_own).astype(jnp.bfloat16)


def solution(mesh):
    split = Mesh(mesh.devices.reshape(8, 4, 2, mesh.shape["tp"]), ("sp_0", "sp_1", "sp_2", "tp"))
    in_specs = (
        P(SP, "tp"),
        P(SP, "tp"),
        P(SP, "tp"),
        P(SP, "tp"),
        P(SP, "tp"),
        P(SP, "tp"),
        P(SP, "tp"),
        P("tp"),
        P("tp", None),
        P(),
        P(SP, "tp"),
        P(SP, "tp"),
        P("tp", SP),
    )
    out_specs = P(SP, "tp")
    return jax.shard_map(local, mesh=split, in_specs=in_specs, out_specs=out_specs, check_vma=False)
```

profile of v0, /device:TPU:1, one launch (start us, length us, event | category | flops | bytes accessed | tf_op | source)
XLA Modules:
  0.0 230.6 jit_solution(16289289867176333970)
XLA Ops:
  6.6 0.8 fusion.83
  7.5 0.5 reduce_window_sum.13
  8.1 0.8 reshape.3324
  9.1 0.9 reshape.3322
  10.0 1.0 reshape.3325
  11.0 0.5 convolution_bitcast_fusion
  11.8 2.1 while.25
  11.9 0.7 bitcast_dynamic-update-slice_fusion.2
  13.0 0.7 bitcast_dynamic-update-slice_fusion.2
  14.0 0.5 copy-done.58
  14.5 5.0 %all-gather.3 = f32[2,259,256]{2,1,0:T(8,128)S(1)} all-gather(f32[1,259,256]{2,1,0:T(8,128)S(1)} %maximum_bitcast_fusion), channel_id=2, replica_groups=mesh['sp_0'=8,'sp_1'=4,'sp_2'=2,'tp'=4] {'sp_2'}, dimensions={0}, use_global_device_ids=true | all-gather | bytes 795648 | tf_op jit(solution)/shard_map/all_gather | solution.py:43
  20.7 0.7 maximum_bitcast_fusion.1
  21.5 25.7 %all-gather.12.cloned.1.call-done = f32[4,259,256]{2,1,0:T(8,128)} async-done(((f32[1,259,256]{2,1,0:T(8,128)}), f32[4,259,256]{2,1,0:T(8,128)}) %all-gather.12.cloned.1.call-update) | async-done | bytes 1060880 | tf_op jit(solution)/shard_map/all_gather | solution.py:43
  47.2 0.8 fusion.155
  48.9 1.5 fusion.43
  51.0 0.8 fusion.86
  51.8 0.7 maximum_bitcast_fusion.2
  52.6 0.8 pad_maximum_fusion
  53.5 0.7 mul.1143
  54.2 0.7 fusion.64
  55.0 0.6 fusion.156
  55.7 1.4 fusion.153
  57.0 2.0 fusion.154
  59.0 33.0 %all-gather.14.cloned.1.call-done = f32[8,259,256]{2,1,0:T(8,128)} async-done(((f32[1,259,256]{2,1,0:T(8,128)}), f32[8,259,256]{2,1,0:T(8,128)}) %all-gather.14.cloned.1.call-update) | async-done | bytes 2121744 | tf_op jit(solution)/shard_map/all_gather | solution.py:43
  92.0 0.9 fusion.152
  93.0 0.6 subtract_exponential_fusion.22
  93.6 0.8 fusion.97
  94.5 1.2 subtract_exponential_fusion.23
  95.7 0.6 copy-done.21
  96.3 1.3 fusion.85
  97.5 1.3 copy.70
  98.8 1.3 add_maximum_fusion.1
  100.1 1.3 copy.72
  101.5 0.7 fusion.84
  102.1 0.7 subtract_exponential_fusion.7
  102.8 0.7 add_maximum_fusion
  103.6 0.7 subtract_exponential_fusion.12
  104.3 0.8 fusion.150
  105.1 1.0 subtract_exponential_fusion.21
  106.1 0.9 multiply_add_fusion.1
  107.0 0.7 fusion.79
  107.8 1.2 fusion.55
  109.0 1.2 fusion.159
  110.2 0.8 subtract_exponential_fusion.2
  111.0 0.3 convolution_bitcast_fusion.2
  111.5 1.6 fusion.151
  113.3 0.8 multiply_add_fusion
  114.3 0.7 multiply_reduce_fusion
  115.0 0.6 broadcast_in_dim.49
  115.6 3.7 %all-to-all-start = ((f32[4,1,128]{2,1,0:T(1,128)}), f32[4,1,128]{2,1,0:T(1,128)S(1)}, u32[]{:S(2)}, u32[]{:S(2)}) async-start(f32[4,1,128]{2,1,0:T(1,128)} %broadcast_in_dim.49), calls=%async_computation | async-start | bytes 4096 | tf_op jit(solution)/shard_map/all_to_all | solution.py:69
  119.3 0.2 copy.74
  119.5 3.8 %all-to-all-done = f32[4,1,128]{2,1,0:T(1,128)S(1)} async-done(((f32[4,1,128]{2,1,0:T(1,128)}), f32[4,1,128]{2,1,0:T(1,128)S(1)}, u32[]{:S(2)}, u32[]{:S(2)}) %all-to-all-start) | async-done | bytes 2080 | tf_op jit(solution)/shard_map/all_to_all | solution.py:69
  123.4 0.5 convolution_convert_fusion
  124.0 9.3 %all_to_all.27 = bf16[4,128,512]{2,1,0:T(8,128)(2,1)S(1)} all-to-all(bf16[4,128,512]{2,1,0:T(8,128)(2,1)S(1)} %bitcast.624), channel_id=1, replica_groups=mesh['sp_0'=8,'sp_1'=4,'sp_2'=2,'tp'=4] {'tp'}, dimensions={0} | all-to-all | bytes 1048576 | tf_op jit(solution)/shard_map/all_to_all | solution.py:85
  133.5 0.6 broadcast_in_dim.50
  134.1 3.2 %all-to-all-start.2 = ((f32[4,1,128]{2,1,0:T(1,128)}), f32[4,1,128]{2,1,0:T(1,128)S(1)}, u32[]{:S(2)}, u32[]{:S(2)}) async-start(f32[4,1,128]{2,1,0:T(1,128)} %broadcast_in_dim.50), calls=%async_computation.2 | async-start | bytes 4096 | tf_op jit(solution)/shard_map/all_to_all | solution.py:69
  137.3 0.8 dynamic_slice.18
  138.1 3.3 %all-to-all-done.2 = f32[4,1,128]{2,1,0:T(1,128)S(1)} async-done(((f32[4,1,128]{2,1,0:T(1,128)}), f32[4,1,128]{2,1,0:T(1,128)S(1)}, u32[]{:S(2)}, u32[]{:S(2)}) %all-to-all-start.2) | async-done | bytes 2080 | tf_op jit(solution)/shard_map/all_to_all | solution.py:69
  141.7 9.3 %all_to_all.28 = bf16[4,128,512]{1,2,0:T(8,128)(2,1)S(1)} all-to-all(bf16[4,128,512]{1,2,0:T(8,128)(2,1)S(1)} %broadcast_in_dim.51), channel_id=1, replica_groups=mesh['sp_0'=8,'sp_1'=4,'sp_2'=2,'tp'=4] {'tp'}, dimensions={0} | all-to-all | bytes 1048576 | tf_op jit(solution)/shard_map/all_to_all | solution.py:69
  151.0 47.5 %all-gather.10.cloned.1.call-done = bf16[2048,4224]{1,0:T(8,128)(2,1)} async-done(((bf16[32,4224]{1,0:T(8,128)(2,1)}), bf16[2048,4224]{1,0:T(8,128)(2,1)}) %all-gather.10.cloned.1.call-update) | async-done | bytes 17301520 | tf_op jit(solution)/shard_map/all_gather | solution.py:21
  198.5 4.5 %fusion.15 = f32[128,1408]{1,0:T(8,128)} fusion(bf16[128,2048]{0,1:T(8,128)(2,1)S(1)} %bitcast.641, bf16[2048,4224]{1,0:T(8,128)(2,1)} %all-gather.10.cloned.1.call-done), kind=kOutput, calls=%fused_computation.26 | convolution fusion | flops 738197504 | bytes 7012352 | tf_op jit(solution)/shard_map/dot_general | solution.py:230
  203.0 7.4 %fusion.20 = bf16[128,2048]{1,0:T(8,128)(2,1)S(1)} fusion(bf16[2048,4224]{1,0:T(8,128)(2,1)} %all-gather.10.cloned.1.call-done, bf16[128,2048]{0,1:T(8,128)(2,1)S(1)} %bitcast.642, f32[128,1408]{1,0:T(8,128)} %fusion.15), kind=kOutput, calls=%fused_computation.29 | convolution fusion | flops 1477738496 | bytes 13303808 | tf_op jit(solution)/shard_map/dot_general | solution.py:233
  210.5 12.8 %all_to_all.29 = bf16[4,128,512]{2,1,0:T(8,128)(2,1)S(1)} all-to-all(bf16[4,128,512]{2,1,0:T(8,128)(2,1)S(1)} %bitcast.625), channel_id=1, replica_groups=mesh['sp_0'=8,'sp_1'=4,'sp_2'=2,'tp'=4] {'tp'}, dimensions={0} | all-to-all | bytes 1048576 | tf_op jit(solution)/shard_map/all_to_all | solution.py:85
  223.4 0.7 fusion.42
  (232 shorter events, 4.9 us)
Async XLA Ops:
  6.5 116.8 %copy-start = (bf16[512,2048]{1,0:T(8,128)(2,1)S(1)}, bf16[512,2048]{1,0:T(8,128)(2,1)}, u32[]{:S(2)}) copy-start(bf16[512,2048]{1,0:T(8,128)(2,1)} %param.23) | copy-start | bytes 6291460
  6.5 40.7 %all-gather.12.cloned.1.call-start = ((), (), s32[]{:S(2)}) async-start(), calls=%async_computation.6 | async-start | bytes 1351680 | tf_op jit(solution)/shard_map/all_gather | solution.py:43
  8.0 46.2 %copy-start.5 = (f32[2,2,64]{2,1,0:T(2,128)}, f32[2,2,64]{2,1,0:T(2,128)S(1)}, u32[]{:S(2)}) copy-start(f32[2,2,64]{2,1,0:T(2,128)S(1)} %reduce_window_sum.13) | copy-start | bytes 3076
  8.9 45.3 %copy-start.13 = (f32[2,64,2]{1,0,2:T(2,128)}, f32[2,64,2]{1,0,2:T(2,128)S(1)}, u32[]{:S(2)}) copy-start(f32[2,64,2]{1,0,2:T(2,128)S(1)} %reshape.3324) | copy-start | bytes 3076
  10.0 1.8 copy-start.3
  14.0 5.6 %copy-start.57 = (f32[2,2]{1,0:T(2,128)}, f32[2,2]{1,0:T(2,128)S(1)}, u32[]{:S(2)}) copy-start(f32[2,2]{1,0:T(2,128)S(1)} %get-tuple-element.79) | copy-start | bytes 52
  14.0 6.0 %copy-start.16 = (f32[2,2]{1,0:T(2,128)}, f32[2,2]{1,0:T(2,128)S(1)}, u32[]{:S(2)}) copy-start(f32[2,2]{1,0:T(2,128)S(1)} %get-tuple-element.84) | copy-start | bytes 52
  19.5 33.0 %copy-start.7 = (bf16[1408,32]{0,1:T(8,128)(2,1)S(1)}, bf16[1408,32]{0,1:T(8,128)(2,1)}, u32[]{:S(2)}) copy-start(bf16[1408,32]{0,1:T(8,128)(2,1)} %param.27) | copy-start | bytes 270340
  19.5 33.1 %copy-start.8 = (bf16[32,1408]{1,0:T(8,128)(2,1)S(1)}, bf16[32,1408]{1,0:T(8,128)(2,1)}, u32[]{:S(2)}) copy-start(bf16[32,1408]{1,0:T(8,128)(2,1)} %param.26) | copy-start | bytes 270340
  19.5 33.1 %copy-start.9 = (bf16[32,1408]{1,0:T(8,128)(2,1)S(1)}, bf16[32,1408]{1,0:T(8,128)(2,1)}, u32[]{:S(2)}) copy-start(bf16[32,1408]{1,0:T(8,128)(2,1)} %param.25) | copy-start | bytes 270340
  19.6 1.9 copy-start.44
  19.7 1.9 copy-start.48
  19.7 28.4 %copy-start.50 = (f32[2]{0:T(128)}, f32[2]{0:T(128)S(1)}, u32[]{:S(2)}) copy-start(f32[2]{0:T(128)S(1)} %get-tuple-element.309) | copy-start | bytes 28
  19.7 1.0 copy-start.59
  20.4 33.1 %copy-start.10 = (bf16[128,256]{1,0:T(8,128)(2,1)S(1)}, bf16[128,256]{1,0:T(8,128)(2,1)}, u32[]{:S(2)}) copy-start(bf16[128,256]{1,0:T(8,128)(2,1)} %param.16) | copy-start | bytes 196612
  21.5 70.5 %all-gather.14.cloned.1.call-start = ((), (), s32[]{:S(2)}) async-start(), calls=%async_computation.7 | async-start | bytes 2433024 | tf_op jit(solution)/shard_map/all_gather | solution.py:43
  48.1 6.8 %copy-start.15 = (f32[4,1,256]{2,0,1:T(4,128)}, f32[4,1,256]{2,0,1:T(4,128)S(1)}, u32[]{:S(2)}) copy-start(f32[4,1,256]{2,0,1:T(4,128)S(1)} %copy.153) | copy-start | bytes 12292
  48.1 2.8 %copy-start.46 = (f32[2]{0:T(128)}, f32[2]{0:T(128)S(1)}, u32[]{:S(2)}) copy-start(f32[2]{0:T(128)S(1)} %get-tuple-element.240) | copy-start | bytes 28
  48.1 6.8 %copy-start.27 = (f32[2]{0:T(128)}, f32[2]{0:T(128)S(1)}, u32[]{:S(2)}) copy-start(f32[2]{0:T(128)S(1)} %get-tuple-element.241) | copy-start | bytes 28
  48.2 6.8 %copy-start.23 = (f32[2]{0:T(128)}, f32[2]{0:T(128)S(1)}, u32[]{:S(2)}) copy-start(f32[2]{0:T(128)S(1)} %get-tuple-element.243) | copy-start | bytes 28
  48.2 6.8 %copy-start.34 = (f32[2]{0:T(128)}, f32[2]{0:T(128)S(1)}, u32[]{:S(2)}) copy-start(f32[2]{0:T(128)S(1)} %get-tuple-element.242) | copy-start | bytes 28
  48.2 6.8 %copy-start.36 = (f32[2]{0:T(128)}, f32[2]{0:T(128)S(1)}, u32[]{:S(2)}) copy-start(f32[2]{0:T(128)S(1)} %get-tuple-element.305) | copy-start | bytes 28
  48.2 2.5 %copy-start.40 = (f32[2]{0:T(128)}, f32[2]{0:T(128)S(1)}, u32[]{:S(2)}) copy-start(f32[2]{0:T(128)S(1)} %get-tuple-element.306) | copy-start | bytes 28
  48.2 6.7 %copy-start.28 = (f32[2]{0:T(128)}, f32[2]{0:T(128)S(1)}, u32[]{:S(2)}) copy-start(f32[2]{0:T(128)S(1)} %get-tuple-element.245) | copy-start | bytes 28
  48.2 6.7 %copy-start.38 = (f32[2]{0:T(128)}, f32[2]{0:T(128)S(1)}, u32[]{:S(2)}) copy-start(f32[2]{0:T(128)S(1)} %get-tuple-element.244) | copy-start | bytes 28
  48.3 2.7 %copy-start.52 = (f32[2]{0:T(128)}, f32[2]{0:T(128)S(1)}, u32[]{:S(2)}) copy-start(f32[2]{0:T(128)S(1)} %get-tuple-element.246) | copy-start | bytes 28
  48.3 2.7 %copy-start.54 = (f32[2]{0:T(128)}, f32[2]{0:T(128)S(1)}, u32[]{:S(2)}) copy-start(f32[2]{0:T(128)S(1)} %get-tuple-element.307) | copy-start | bytes 28
  48.3 6.7 %copy-start.32 = (f32[2]{0:T(128)}, f32[2]{0:T(128)S(1)}, u32[]{:S(2)}) copy-start(f32[2]{0:T(128)S(1)} %get-tuple-element.247) | copy-start | bytes 28
  48.3 6.7 %copy-start.33 = (f32[2]{0:T(128)}, f32[2]{0:T(128)S(1)}, u32[]{:S(2)}) copy-start(f32[2]{0:T(128)S(1)} %get-tuple-element.308) | copy-start | bytes 28
  48.3 3.4 %copy-start.61 = (f32[2]{0:T(128)}, f32[2]{0:T(128)S(1)}, u32[]{:S(2)}) copy-start(f32[2]{0:T(128)S(1)} %subtract_exponential_fusion.24) | copy-start | bytes 28
  52.5 146.0 %all-gather.10.cloned.1.call-start = ((), (), s32[]{:S(2)}) async-start(), calls=%async_computation.5 | async-start | bytes 17571840 | tf_op jit(solution)/shard_map/all_gather | solution.py:21
  54.2 0.8 copy-start.12
  55.6 47.2 %copy-start.6 = (f32[2,2,64]{2,1,0:T(2,128)S(1)}, f32[2,2,64]{2,1,0:T(2,128)}, u32[]{:S(2)}) copy-start(f32[2,2,64]{2,1,0:T(2,128)} %copy-done.5) | copy-start | bytes 3076
  55.7 53.3 %copy-start.14 = (f32[2,64,2]{1,0,2:T(2,128)S(1)}, f32[2,64,2]{1,0,2:T(2,128)}, u32[]{:S(2)}) copy-start(f32[2,64,2]{1,0,2:T(2,128)} %copy-done.13) | copy-start | bytes 3076
  93.6 0.9 copy-start.17
  93.6 0.9 copy-start.18
  93.6 0.9 copy-start.19
  93.6 2.1 copy-start.20
  93.6 3.9 %copy-start.24 = (f32[2]{0:T(128)}, f32[2]{0:T(128)S(1)}, u32[]{:S(2)}) copy-start(f32[2]{0:T(128)S(1)} %get-tuple-element.235) | copy-start | bytes 28
  93.6 3.9 %copy-start.25 = (f32[2]{0:T(128)}, f32[2]{0:T(128)S(1)}, u32[]{:S(2)}) copy-start(f32[2]{0:T(128)S(1)} %get-tuple-element.236) | copy-start | bytes 28
  93.6 3.9 %copy-start.26 = (f32[2]{0:T(128)}, f32[2]{0:T(128)S(1)}, u32[]{:S(2)}) copy-start(f32[2]{0:T(128)S(1)} %get-tuple-element.237) | copy-start | bytes 28
  111.3 1.8 copy-start.1
  111.4 1.8 copy-start.35
  111.4 1.8 copy-start.37
  111.4 1.8 copy-start.39
  111.4 1.8 copy-start.41
  111.4 1.8 copy-start.42
  111.4 1.8 copy-start.43
  111.4 1.8 copy-start.45
  111.4 1.8 copy-start.47
  111.4 1.8 copy-start.49
  111.4 1.8 copy-start.51
  111.5 1.8 copy-start.53
  111.5 1.8 copy-start.55
  111.5 1.8 copy-start.60
  111.5 1.8 copy-start.62
  113.1 1.0 copy-start.2
  113.2 1.0 copy-start.56
  113.2 1.1 copy-start.63
  114.2 9.2 %copy-start.64 = (bf16[128,512]{1,0:T(8,128)(2,1)S(1)}, bf16[128,512]{1,0:T(8,128)(2,1)}, u32[]{:S(2)}) copy-start(bf16[128,512]{1,0:T(8,128)(2,1)} %param.19) | copy-start | bytes 393220
  114.2 9.2 %copy-start.65 = (f32[512]{0:T(512)S(1)}, f32[512]{0:T(512)}, u32[]{:S(2)}) copy-start(f32[512]{0:T(512)} %param.22) | copy-start | bytes 6148
  115.6 7.7 %all-to-all-start = ((f32[4,1,128]{2,1,0:T(1,128)}), f32[4,1,128]{2,1,0:T(1,128)S(1)}, u32[]{:S(2)}, u32[]{:S(2)}) async-start(f32[4,1,128]{2,1,0:T(1,128)} %broadcast_in_dim.49), calls=%async_computation | async-start | bytes 4096 | tf_op jit(solution)/shard_map/all_to_all | solution.py:69
  123.9 9.5 %copy-start.4 = (bf16[128,512]{1,0:T(8,128)(2,1)S(1)}, bf16[128,512]{1,0:T(8,128)(2,1)}, u32[]{:S(2)}) copy-start(bf16[128,512]{1,0:T(8,128)(2,1)} %param.15) | copy-start | bytes 393220
  134.1 7.3 %all-to-all-start.2 = ((f32[4,1,128]{2,1,0:T(1,128)}), f32[4,1,128]{2,1,0:T(1,128)S(1)}, u32[]{:S(2)}, u32[]{:S(2)}) async-start(f32[4,1,128]{2,1,0:T(1,128)} %broadcast_in_dim.50), calls=%async_computation.2 | async-start | bytes 4096 | tf_op jit(solution)/shard_map/all_to_all | solution.py:69
  (7 other events, 4.0 us)
Sparse Core Ops, SparseCore 0:
  21.6 25.6 all-gather.11
  52.7 39.3 all-gather.13
  94.7 103.7 all-gather.9
where the time goes:
time: 232 us; the launch traced here: 231 us
  waiting for transfers between devices  113 us (49%)
  blocking collectives  36.5 us (16%)
  other arithmetic  22.5 us (10%)
  local copies, waits for them, and re-layouts  20.5 us (9%)
  matrix products  16.5 us (7%)
  between operations  14.3 us (6%)
  starting transfers between devices  6.98 us (3%)
    all_gather x2, waiting for transfers between devices, all_in_one(): both, at, found = (lax.all_gather(jnp.concatenate(lines), axis), 0, {})  58.7 us
    all_gather x1, waiting for transfers between devices, gather_turned(): lax.all_gather(both, axis, axis=0, tiled=True)  47.5 us
    all_to_all x2, blocking collectives, summed_on_arrival(): lax.all_to_all(parts, axis, split_axis=0, concat_axis=0, tiled=True)  22.1 us
    all_to_all x1, blocking collectives, copy_for_each(): lax.all_to_all(jnp.broadcast_to(x[None], (peers, *x.shape)), axis, 0, 0,...  9.34 us
    dot_general x1, matrix products, local(): term = jnp.dot(hidden, down_full, preferred_element_type=jnp.float32)  7.41 us
    all_to_all x2, waiting for transfers between devices, copy_for_each(): lax.all_to_all(jnp.broadcast_to(x[None], (peers, *x.shape)), axis, 0, 0,...  7.08 us
    all_to_all x2, starting transfers between devices, copy_for_each(): lax.all_to_all(jnp.broadcast_to(x[None], (peers, *x.shape)), axis, 0, 0,...  6.89 us
    slice x6, local copies, waits for them, and re-layouts, entering(): subtotal = combine(subtotal, jax.tree.map(lambda part: part[k], pieces))  6.41 us
  transfers between devices with their start and end apart: 5, of which 5 were waited for; matrix products, arithmetic and copies ran while one was open for 14% of the time, Pallas kernels for 0%

commit v1 on v0

--- a/solution.py
+++ b/solution.py
@@ -18,7 +18,13 @@
 def gather_turned(arrays, axis, dims):
     turned = [jnp.moveaxis(a, dim, 0) for a, dim in zip(arrays, dims)]
     both = jnp.concatenate([t.reshape(len(t), -1) for t in turned], axis=1)
-    result, at, gathered = (lax.all_gather(both, axis, axis=0, tiled=True), 0, [])
+    result, at, gathered = (
+        jnp.concatenate(
+            lax.all_to_all(jnp.stack([both] * lax.axis_size(axis)), axis, 0, 0), axis=0
+        ),
+        0,
+        [],
+    )
     for t, dim in zip(turned, dims):
         slab = result[:, at : at + t[0].size].reshape(-1, *t.shape[1:])
         gathered.append(jnp.moveaxis(slab, 0, dim))

time: 232 us -> 584 us (2.52)
  blocking collectives: 36.5 us -> 421 us
  waiting for transfers between devices: 113 us -> 73.5 us
  local copies, waits for them, and re-layouts: 20.5 us -> 27.2 us
    all_to_all x1, blocking collectives: 9.34 us -> 395 us  [gather_turned(): lax.all_to_all(jnp.stack([both] * lax.axis_size(axis)), axis, 0, 0)]
    all_gather x1 -> x0, waiting for transfers between devices: 47.5 us -> none  [gather_turned(): lax.all_gather(both, axis, axis=0, tiled=True)]
    all_to_all x2 -> x3, waiting for transfers between devices: 7.08 us -> 13.9 us  [copy_for_each(): lax.all_to_all(jnp.broadcast_to(x[None], (peers, *x.shape)), axis, 0, 0,...]
  transfers between devices with their start and end apart: 5 -> 5, of which waited for: 5 -> 5; matrix products, arithmetic and copies ran while one was open for 14% -> 1% of each run, Pallas kernels for 0% -> 0%
where the time goes in v1:
time: 584 us; the launch traced here: 583 us
  blocking collectives  421 us (72%)
  waiting for transfers between devices  73.5 us (13%)
  local copies, waits for them, and re-layouts  27.2 us (5%)
  other arithmetic  22.4 us (4%)
  matrix products  14.8 us (3%)
  between operations  14.4 us (2%)
  starting transfers between devices  10.4 us (2%)
    all_to_all x1, blocking collectives, gather_turned(): lax.all_to_all(jnp.stack([both] * lax.axis_size(axis)), axis, 0, 0)  395 us
    all_gather x2, waiting for transfers between devices, all_in_one(): both, at, found = (lax.all_gather(jnp.concatenate(lines), axis), 0, {})  59.5 us
    all_to_all x2, blocking collectives, summed_on_arrival(): lax.all_to_all(parts, axis, split_axis=0, concat_axis=0, tiled=True)  21 us
    all_to_all x3, waiting for transfers between devices, copy_for_each(): lax.all_to_all(jnp.broadcast_to(x[None], (peers, *x.shape)), axis, 0, 0,...  13.9 us
  transfers between devices with their start and end apart: 5, of which 5 were waited for; matrix products, arithmetic and copies ran while one was open for 1% of the time, Pallas kernels for 0%

profile of v1, /device:TPU:1, one launch (start us, length us, event | category | flops | bytes accessed | tf_op | source)
XLA Modules:
  0.0 583.2 jit_solution(15405251119930633748)
XLA Ops:
  6.6 0.8 fusion.83
  7.5 0.8 reshape.3329
  8.3 0.5 reduce_window_sum.13
  9.3 0.9 reshape.3330
  10.3 0.9 reshape.3327
  11.2 0.5 convolution_bitcast_fusion
  11.8 2.1 while.25
  11.8 0.7 bitcast_dynamic-update-slice_fusion.2
  12.9 0.7 bitcast_dynamic-update-slice_fusion.2
  14.0 5.0 all-gather.3
  19.9 0.7 maximum_bitcast_fusion.1
  20.8 25.7 %all-gather.9.cloned.1.call-done = f32[4,259,256]{2,1,0:T(8,128)} async-done(((f32[1,259,256]{2,1,0:T(8,128)}), f32[4,259,256]{2,1,0:T(8,128)}) %all-gather.9.cloned.1.call-update) | async-done | bytes 1060880 | tf_op jit(solution)/shard_map/all_gather | solution.py:49
  46.5 0.8 fusion.155
  48.7 0.8 fusion.86
  49.5 1.5 fusion.43
  51.0 0.7 maximum_bitcast_fusion.2
  51.9 0.7 mul.1143
  52.7 0.7 fusion.64
  53.5 0.6 fusion.156
  54.1 1.3 fusion.153
  55.5 2.0 fusion.154
  57.5 33.8 %all-gather.11.cloned.1.call-done = f32[8,259,256]{2,1,0:T(8,128)} async-done(((f32[1,259,256]{2,1,0:T(8,128)}), f32[8,259,256]{2,1,0:T(8,128)}) %all-gather.11.cloned.1.call-update) | async-done | bytes 2121744 | tf_op jit(solution)/shard_map/all_gather | solution.py:49
  91.3 0.9 fusion.152
  92.2 0.6 subtract_exponential_fusion.22
  92.8 0.8 fusion.97
  93.6 1.2 subtract_exponential_fusion.23
  94.8 1.3 add_maximum_fusion.1
  96.1 1.3 fusion.85
  97.4 0.6 subtract_exponential_fusion.21
  98.0 0.6 subtract_exponential_fusion.12
  98.6 0.7 fusion.84
  99.3 1.3 copy.70
  100.6 1.3 copy.72
  102.0 0.8 subtract_exponential_fusion.7
  102.7 0.8 fusion.150
  103.6 1.0 multiply_add_fusion.1
  104.5 0.7 fusion.79
  105.3 1.2 fusion.55
  106.5 0.8 add_maximum_fusion
  107.3 1.2 fusion.159
  108.5 0.3 convolution_bitcast_fusion.2
  108.8 0.8 subtract_exponential_fusion.2
  109.6 1.6 fusion.151
  111.3 1.9 multiply_add_fusion
  113.3 0.7 multiply_reduce_fusion
  114.0 0.6 broadcast_in_dim.49
  114.6 3.7 all-to-all-start
  118.5 3.8 all-to-all-done
  122.4 1.4 convolution_convert_fusion
  123.9 9.3 %all_to_all.32 = bf16[4,128,512]{2,1,0:T(8,128)(2,1)S(1)} all-to-all(bf16[4,128,512]{2,1,0:T(8,128)(2,1)S(1)} %bitcast.627), channel_id=1, replica_groups=mesh['sp_0'=8,'sp_1'=4,'sp_2'=2,'tp'=4] {'tp'}, dimensions={0} | all-to-all | bytes 1048576 | tf_op jit(solution)/shard_map/all_to_all | solution.py:91
  133.4 0.6 broadcast_in_dim.50
  134.0 3.2 all-to-all-start.2
  137.2 0.8 dynamic_slice.18
  138.0 3.3 all-to-all-done.2
  141.5 0.9 broadcast_in_dim.51
  142.4 3.5 all-to-all-start.3
  145.9 6.8 %all-to-all-done.3 = bf16[4,128,512]{1,2,0:T(8,128)(2,1)S(1)} async-done(((bf16[4,128,512]{1,2,0:T(8,128)(2,1)}), bf16[4,128,512]{1,2,0:T(8,128)(2,1)S(1)}, u32[]{:S(2)}, u32[]{:S(2)}) %all-to-all-start.3) | async-done | bytes 524320 | tf_op jit(solution)/shard_map/all_to_all | solution.py:75
  152.8 1.3 stack.2
  154.1 394.5 %all_to_all.33 = bf16[64,32,4224]{2,1,0:T(8,128)(2,1)S(1)} all-to-all(bf16[64,32,4224]{2,1,0:T(8,128)(2,1)S(1)} %stack.2), channel_id=1, replica_groups=mesh['sp_0'=8,'sp_1'=4,'sp_2'=2,'tp'=4] {'sp_0','sp_1','sp_2'}, dimensions={0} | all-to-all | bytes 34603008 | tf_op jit(solution)/shard_map/all_to_all | solution.py:23
  548.6 6.0 %copy-done.1 = bf16[64,32,4224]{2,1,0:T(8,128)(2,1)} copy-done((bf16[64,32,4224]{2,1,0:T(8,128)(2,1)}, bf16[64,32,4224]{2,1,0:T(8,128)(2,1)S(1)}, u32[]{:S(2)}) %copy-start.1) | copy-done | bytes 17301528
  554.6 1.9 fusion.15
  556.5 7.4 %fusion.20 = bf16[128,2048]{1,0:T(8,128)(2,1)S(1)} fusion(bf16[2048,4224]{1,0:T(8,128)(2,1)} %bitcast.626, bf16[128,2048]{0,1:T(8,128)(2,1)S(1)} %bitcast.645, f32[128,1408]{1,0:T(8,128)} %fusion.15), kind=kOutput, calls=%fused_computation.29 | convolution fusion | flops 1477738496 | bytes 13303808 | tf_op jit(solution)/shard_map/dot_general | solution.py:239
  563.9 11.7 %all_to_all.34 = bf16[4,128,512]{2,1,0:T(8,128)(2,1)S(1)} all-to-all(bf16[4,128,512]{2,1,0:T(8,128)(2,1)S(1)} %bitcast.628), channel_id=1, replica_groups=mesh['sp_0'=8,'sp_1'=4,'sp_2'=2,'tp'=4] {'tp'}, dimensions={0} | all-to-all | bytes 1048576 | tf_op jit(solution)/shard_map/all_to_all | solution.py:91
  575.7 0.7 fusion.42
  (188 shorter events, 4.7 us)
Async XLA Ops:
  6.5 115.9 %copy-start = (bf16[512,2048]{1,0:T(8,128)(2,1)S(1)}, bf16[512,2048]{1,0:T(8,128)(2,1)}, u32[]{:S(2)}) copy-start(bf16[512,2048]{1,0:T(8,128)(2,1)} %param.23) | copy-start | bytes 6291460
  6.5 39.9 %all-gather.9.cloned.1.call-start = ((), (), s32[]{:S(2)}) async-start(), calls=%async_computation.6 | async-start | bytes 1351680 | tf_op jit(solution)/shard_map/all_gather | solution.py:49
  8.3 44.4 %copy-start.11 = (f32[2,64,2]{1,0,2:T(2,128)}, f32[2,64,2]{1,0,2:T(2,128)S(1)}, u32[]{:S(2)}) copy-start(f32[2,64,2]{1,0,2:T(2,128)S(1)} %reshape.3329) | copy-start | bytes 3076
  8.7 43.9 %copy-start.5 = (f32[2,2,64]{2,1,0:T(2,128)}, f32[2,2,64]{2,1,0:T(2,128)S(1)}, u32[]{:S(2)}) copy-start(f32[2,2,64]{2,1,0:T(2,128)S(1)} %reduce_window_sum.13) | copy-start | bytes 3076
  11.1 39.9 %copy-start.3 = (bf16[2,64,2,128]{3,2,1,0:T(2,128)(2,1)}, bf16[2,64,2,128]{3,2,1,0:T(2,128)(2,1)S(1)}, u32[]{:S(2)}) copy-start(bf16[2,64,2,128]{3,2,1,0:T(2,128)(2,1)S(1)} %reshape.3327) | copy-start | bytes 196612
  11.8 40.1 %copy-start.9 = (bf16[128,256]{1,0:T(8,128)(2,1)S(1)}, bf16[128,256]{1,0:T(8,128)(2,1)}, u32[]{:S(2)}) copy-start(bf16[128,256]{1,0:T(8,128)(2,1)} %param.16) | copy-start | bytes 196612
  13.9 39.5 %copy-start.13 = (f32[2,2]{1,0:T(2,128)}, f32[2,2]{1,0:T(2,128)S(1)}, u32[]{:S(2)}) copy-start(f32[2,2]{1,0:T(2,128)S(1)} %get-tuple-element.84) | copy-start | bytes 52
  13.9 39.5 %copy-start.38 = (f32[2,2]{1,0:T(2,128)}, f32[2,2]{1,0:T(2,128)S(1)}, u32[]{:S(2)}) copy-start(f32[2,2]{1,0:T(2,128)S(1)} %get-tuple-element.79) | copy-start | bytes 52
  13.9 39.5 %copy-start.39 = (f32[2,2,128]{2,1,0:T(2,128)}, f32[2,2,128]{2,1,0:T(2,128)S(1)}, u32[]{:S(2)}) copy-start(f32[2,2,128]{2,1,0:T(2,128)S(1)} %get-tuple-element.86) | copy-start | bytes 6148
  19.0 1.7 copy-start.16
  19.0 1.7 copy-start.20
  19.0 28.4 %copy-start.29 = (f32[2]{0:T(128)}, f32[2]{0:T(128)S(1)}, u32[]{:S(2)}) copy-start(f32[2]{0:T(128)S(1)} %get-tuple-element.248) | copy-start | bytes 28
  19.1 28.2 %copy-start.21 = (f32[2]{0:T(128)}, f32[2]{0:T(128)S(1)}, u32[]{:S(2)}) copy-start(f32[2]{0:T(128)S(1)} %get-tuple-element.251) | copy-start | bytes 28
  19.1 28.3 %copy-start.22 = (f32[2]{0:T(128)}, f32[2]{0:T(128)S(1)}, u32[]{:S(2)}) copy-start(f32[2]{0:T(128)S(1)} %get-tuple-element.310) | copy-start | bytes 28
  19.1 28.3 %copy-start.32 = (f32[2]{0:T(128)}, f32[2]{0:T(128)S(1)}, u32[]{:S(2)}) copy-start(f32[2]{0:T(128)S(1)} %get-tuple-element.309) | copy-start | bytes 28
  19.1 28.4 %copy-start.31 = (f32[2]{0:T(128)}, f32[2]{0:T(128)S(1)}, u32[]{:S(2)}) copy-start(f32[2]{0:T(128)S(1)} %get-tuple-element.250) | copy-start | bytes 28
  19.1 28.3 %copy-start.40 = (f32[2]{0:T(128)}, f32[2]{0:T(128)S(1)}, u32[]{:S(2)}) copy-start(f32[2]{0:T(128)S(1)} %subtract_exponential_fusion.31) | copy-start | bytes 28
  20.7 70.6 %all-gather.11.cloned.1.call-start = ((), (), s32[]{:S(2)}) async-start(), calls=%async_computation.7 | async-start | bytes 2433024 | tf_op jit(solution)/shard_map/all_gather | solution.py:49
  47.3 6.1 %copy-start.12 = (f32[4,1,256]{2,0,1:T(4,128)}, f32[4,1,256]{2,0,1:T(4,128)S(1)}, u32[]{:S(2)}) copy-start(f32[4,1,256]{2,0,1:T(4,128)S(1)} %copy.153) | copy-start | bytes 12292
  47.4 4.5 copy-start.30
  47.4 6.1 %copy-start.18 = (f32[2]{0:T(128)}, f32[2]{0:T(128)S(1)}, u32[]{:S(2)}) copy-start(f32[2]{0:T(128)S(1)} %get-tuple-element.241) | copy-start | bytes 28
  47.4 4.4 copy-start.26
  47.4 6.0 %copy-start.17 = (f32[2]{0:T(128)}, f32[2]{0:T(128)S(1)}, u32[]{:S(2)}) copy-start(f32[2]{0:T(128)S(1)} %get-tuple-element.243) | copy-start | bytes 28
  47.4 6.0 %copy-start.25 = (f32[2]{0:T(128)}, f32[2]{0:T(128)S(1)}, u32[]{:S(2)}) copy-start(f32[2]{0:T(128)S(1)} %get-tuple-element.242) | copy-start | bytes 28
  47.5 4.4 copy-start.27
  47.5 4.4 copy-start.28
  47.5 6.0 %copy-start.19 = (f32[2]{0:T(128)}, f32[2]{0:T(128)S(1)}, u32[]{:S(2)}) copy-start(f32[2]{0:T(128)S(1)} %get-tuple-element.245) | copy-start | bytes 28
  47.5 4.3 copy-start.33
  47.6 4.3 copy-start.34
  47.6 5.9 %copy-start.23 = (f32[2]{0:T(128)}, f32[2]{0:T(128)S(1)}, u32[]{:S(2)}) copy-start(f32[2]{0:T(128)S(1)} %get-tuple-element.247) | copy-start | bytes 28
  47.6 5.9 %copy-start.24 = (f32[2]{0:T(128)}, f32[2]{0:T(128)S(1)}, u32[]{:S(2)}) copy-start(f32[2]{0:T(128)S(1)} %get-tuple-element.308) | copy-start | bytes 28
  47.6 1.1 copy-start.41
  52.7 0.8 copy-start.10
  94.8 3.8 copy-start.15
  97.4 1.2 copy-start.14
  99.3 5.2 copy-start.35
  102.0 11.3 %copy-start.2 = (f32[2,64,2,128]{3,2,1,0:T(2,128)S(1)}, f32[2,64,2,128]{3,2,1,0:T(2,128)}, u32[]{:S(2)}) copy-start(f32[2,64,2,128]{3,2,1,0:T(2,128)} %mul.1143) | copy-start | bytes 393220
  102.0 11.3 %copy-start.37 = (f32[2,2]{0,1:T(2,128)S(1)}, f32[2,2]{0,1:T(2,128)}, u32[]{:S(2)}) copy-start(f32[2,2]{0,1:T(2,128)} %get-tuple-element.224) | copy-start | bytes 52
  102.0 11.3 %copy-start.42 = (f32[2,2,128,256]{3,2,1,0:T(8,128)S(1)}, f32[2,2,128,256]{3,2,1,0:T(8,128)}, u32[]{:S(2)}) copy-start(f32[2,2,128,256]{3,2,1,0:T(8,128)} %get-tuple-element.85) | copy-start | bytes 1572868
  105.3 8.0 %copy-start.36 = (f32[2,2]{0,1:T(2,128)S(1)}, f32[2,2]{0,1:T(2,128)}, u32[]{:S(2)}) copy-start(f32[2,2]{0,1:T(2,128)} %copy-done.35) | copy-start | bytes 52
  108.8 13.6 %copy-start.43 = (f32[512]{0:T(512)S(1)}, f32[512]{0:T(512)}, u32[]{:S(2)}) copy-start(f32[512]{0:T(512)} %param.22) | copy-start | bytes 6148
  113.2 20.1 %copy-start.4 = (bf16[128,512]{1,0:T(8,128)(2,1)S(1)}, bf16[128,512]{1,0:T(8,128)(2,1)}, u32[]{:S(2)}) copy-start(bf16[128,512]{1,0:T(8,128)(2,1)} %param.15) | copy-start | bytes 393220
  113.3 32.6 %copy-start.6 = (bf16[1408,32]{0,1:T(8,128)(2,1)S(1)}, bf16[1408,32]{0,1:T(8,128)(2,1)}, u32[]{:S(2)}) copy-start(bf16[1408,32]{0,1:T(8,128)(2,1)} %param.27) | copy-start | bytes 270340
  113.3 32.6 %copy-start.7 = (bf16[32,1408]{1,0:T(8,128)(2,1)S(1)}, bf16[32,1408]{1,0:T(8,128)(2,1)}, u32[]{:S(2)}) copy-start(bf16[32,1408]{1,0:T(8,128)(2,1)} %param.26) | copy-start | bytes 270340
  113.3 32.6 %copy-start.8 = (bf16[32,1408]{1,0:T(8,128)(2,1)S(1)}, bf16[32,1408]{1,0:T(8,128)(2,1)}, u32[]{:S(2)}) copy-start(bf16[32,1408]{1,0:T(8,128)(2,1)} %param.25) | copy-start | bytes 270340
  114.6 7.7 %all-to-all-start = ((f32[4,1,128]{2,1,0:T(1,128)}), f32[4,1,128]{2,1,0:T(1,128)S(1)}, u32[]{:S(2)}, u32[]{:S(2)}) async-start(f32[4,1,128]{2,1,0:T(1,128)} %broadcast_in_dim.49), calls=%async_computation | async-start | bytes 4096 | tf_op jit(solution)/shard_map/all_to_all | solution.py:75
  134.0 7.3 %all-to-all-start.2 = ((f32[4,1,128]{2,1,0:T(1,128)}), f32[4,1,128]{2,1,0:T(1,128)S(1)}, u32[]{:S(2)}, u32[]{:S(2)}) async-start(f32[4,1,128]{2,1,0:T(1,128)} %broadcast_in_dim.50), calls=%async_computation.2 | async-start | bytes 4096 | tf_op jit(solution)/shard_map/all_to_all | solution.py:75
  142.4 10.4 %all-to-all-start.3 = ((bf16[4,128,512]{1,2,0:T(8,128)(2,1)}), bf16[4,128,512]{1,2,0:T(8,128)(2,1)S(1)}, u32[]{:S(2)}, u32[]{:S(2)}) async-start(bf16[4,128,512]{1,2,0:T(8,128)(2,1)} %broadcast_in_dim.51), calls=%async_computation.3 | async-start | bytes 1048576 | tf_op jit(solution)/shard_map/all_to_all | solution.py:75
  548.6 6.0 %copy-start.1 = (bf16[64,32,4224]{2,1,0:T(8,128)(2,1)}, bf16[64,32,4224]{2,1,0:T(8,128)(2,1)S(1)}, u32[]{:S(2)}) copy-start(bf16[64,32,4224]{2,1,0:T(8,128)(2,1)S(1)} %all_to_all.33) | copy-start | bytes 51904516
Sparse Core Ops, SparseCore 0:
  20.8 25.6 all-gather.8
  51.9 39.3 all-gather.10
